TPU v7x, 32 devices: a whole 2x2x4 slice. The times are simulated.
32 devices in a mesh: sp: 8 (over z, y), tp: 4 (over x, core).
Axes of the slice: x: 2, y: 2, z: 4, core: 2. Of those that a mesh axis runs over, the one named last changes fastest.
Arguments:
- mixer_input: bfloat16 [1024, 1024], P('sp', 'tp'), may hold values from -1800 to 1800
- time_step: float32 [2, 64], P(None, 'tp'), may hold values from 0 to 2, as said below
- damping: float32 [2, 1024, 64], P(None, 'sp', 'tp'), may hold values from 0 to 2
- input_map: bfloat16 [2, 2, 64, 64, 16], P(None, None, 'tp'), may hold values from -1 to 1
- readout: float32 [2, 2, 64, 16, 64], P(None, None, 'tp'), may hold values from -0.5 to 0.5
- skip_gain: float32 [1024], P('tp'), may hold values from -4 to 4
- out_gain: float32 [1024], P('tp'), may hold values from 0.1 to 1.9
- out_weight: bfloat16 [1024, 2048], replicated, may hold values from -0.1875 to 0.1875
- residual: bfloat16 [1024, 2048], P(('sp', 'tp')), may hold values from -6 to 6
- channel_gain: float32 [2048], replicated, may hold values from 0.1 to 1.9
- value_weight: bfloat16 [2048, 6144], P('sp', 'tp'), may hold values from -0.125 to 0.125
- gate_weight: bfloat16 [2048, 6144], P('sp', 'tp'), may hold values from -0.125 to 0.125
- value_taps: float32 [3, 6144], P(None, 'tp'), may hold values from -3 to 3
- gate_taps: float32 [3, 6144], P(None, 'tp'), may hold values from -3 to 3
- down_weight: bfloat16 [6144, 2048], P('tp', 'sp'), may hold values from -0.078125 to 0.078125
Outputs:
- output: bfloat16 [1024, 2048], P(('sp', 'tp'))
Inputs may be any that keep to these rules, and one draw needn't show every extreme that they name: `time_step`: positive.
All inputs are finite; a program needn't handle non-finite values.
Results may differ from a plain program's by a relative error of at most 0.017.
Values may be sent and summed in bfloat16 or wider, within the bound.
A program may use at most 128 MiB of HBM per device.

v0:
```python
import math

import jax
import jax.numpy as jnp
from jax import lax
from jax.experimental import pallas as pl
from jax.experimental.pallas import tpu as pltpu
from jax.sharding import PartitionSpec as P

norm_eps = 1e-06
highest = lax.Precision.HIGHEST
mesh_ids = pl.DeviceIdType.MESH


def carry_kernel(count, own_ref, all_ref, local_sem, send_sem, recv_sem):
    sp, tp = lax.axis_index("sp"), lax.axis_index("tp")
    barrier = pltpu.get_barrier_semaphore()
    for offset in range(1, count):
        peer = lax.rem(sp + offset, count)
        pl.semaphore_signal(barrier, inc=1, device_id=(peer, tp), device_id_type=mesh_ids)
    pl.semaphore_wait(barrier, count - 1)
    keep = pltpu.make_async_copy(own_ref, all_ref.at[sp], local_sem)
    keep.start()
    copies = []
    for offset in range(1, count):
        peer = lax.rem(sp + offset, count)
        copy = pltpu.make_async_remote_copy(
            src_ref=own_ref,
            dst_ref=all_ref.at[sp],
            send_sem=send_sem.at[offset],
            recv_sem=recv_sem.at[offset],
            device_id=(peer, tp),
            device_id_type=mesh_ids,
        )
        copy.start()
        copies.append(copy)
    keep.wait()
    for copy in copies:
        copy.wait()


def gather_ends(packed, count):
    vmem = pl.BlockSpec(memory_space=pltpu.VMEM)
    return pl.pallas_call(
        lambda *refs: carry_kernel(count, *refs),
        name="gather_ends",
        out_shape=jax.ShapeDtypeStruct((count,) + packed.shape, packed.dtype),
        in_specs=[vmem],
        out_specs=vmem,
        scratch_shapes=[
            pltpu.SemaphoreType.DMA,
            pltpu.SemaphoreType.DMA((count,)),
            pltpu.SemaphoreType.DMA((count,)),
        ],
        compiler_params=pltpu.CompilerParams(collective_id=0, has_side_effects=True),
    )(packed)


gather_orders = (("z", "y", "x", "c"), ("y", "z", "x", "c"))
sum_orders = (("c", "x", "y", "z"), ("c", "z", "y", "x"))
axes = ("z", "y", "x", "c")


def channel_kernel(sizes, *refs):
    normed_ref, hidden_state_ref, up_send, down_send, taps_ref, out_ref = refs[:6]
    rows_all, up_rows, partial, up_land, down_land, down_ref = refs[6:12]
    landing = refs[12:20]
    local_sem, send_sem, recv_sem, weight_send_sem, weight_recv_sem = refs[20:25]
    rows, width = normed_ref.shape
    half = width // 2
    count, part, part_width = down_send.shape
    sp, tp = lax.axis_index("sp"), lax.axis_index("tp")
    mine = {
        "z": sp // sizes["y"],
        "y": lax.rem(sp, sizes["y"]),
        "x": tp // sizes["c"],
        "c": lax.rem(tp, sizes["c"]),
    }

    def neighbour(axis, offset):
        at = dict(mine)
        at[axis] = lax.rem(mine[axis] + offset, sizes[axis])
        return at[axis], (at["z"] * sizes["y"] + at["y"], at["x"] * sizes["c"] + at["c"])

    barrier = pltpu.get_barrier_semaphore()
    greeted = 0
    for axis in ("x", "c"):
        for offset in range(1, sizes[axis]):
            _, device = neighbour(axis, offset)
            pl.semaphore_signal(barrier, inc=1, device_id=device, device_id_type=mesh_ids)
            greeted += 1
    for offset in range(1, count):
        peer = lax.rem(sp + offset, count)
        pl.semaphore_signal(barrier, inc=1, device_id=(peer, tp), device_id_type=mesh_ids)
        greeted += 1
    pl.semaphore_wait(barrier, greeted)

    keeps = []
    for kind, (source, target) in enumerate(
        (
            (normed_ref, rows_all.at[mine["z"], mine["y"], mine["x"], mine["c"]]),
            (up_send.at[sp], up_land.at[sp]),
            (down_send.at[sp], down_land.at[sp]),
        )
    ):
        keep = pltpu.make_async_copy(source, target, local_sem.at[kind])
        keep.start()
        keeps.append(keep)
    keeps[0].wait()

    def spread(source, land, kind):
        started = []
        for offset in range(1, count):
            peer = lax.rem(sp + offset, count)
            copy = pltpu.make_async_remote_copy(
                src_ref=source.at[peer],
                dst_ref=land.at[sp],
                send_sem=weight_send_sem.at[kind, offset],
                recv_sem=weight_recv_sem.at[kind, offset],
                device_id=(peer, tp),
                device_id_type=mesh_ids,
            )
            copy.start()
            started.append(copy)
        return started

    slot = 0
    pending = [[], []]
    up_copies, down_copies = [], []
    for stage in range(4):
        if stage == 2:
            up_copies = spread(up_send, up_land, 0)
            down_copies = spread(down_send, down_land, 1)
        for piece in range(2):
            axis = gather_orders[piece][stage]
            done = gather_orders[piece][:stage]
            for copy in pending[piece]:
                copy.wait()
            pending[piece] = []
            index = tuple(slice(None) if name in done else mine[name] for name in axes)
            block = rows_all.at[index + (slice(None), pl.ds(piece * half, half))]
            for offset in range(1, sizes[axis]):
                _, device = neighbour(axis, offset)
                copy = pltpu.make_async_remote_copy(
                    src_ref=block,
                    dst_ref=block,
                    send_sem=send_sem.at[slot],
                    recv_sem=recv_sem.at[slot],
                    device_id=device,
                    device_id_type=mesh_ids,
                )
                copy.start()
                pending[piece].append(copy)
                slot += 1
    for piece in range(2):
        for copy in pending[piece]:
            copy.wait()

    plane = sizes["y"] * sizes["x"] * sizes["c"] * rows
    total = plane * sizes["z"]
    for copy in [keeps[1]] + up_copies:
        copy.wait()
    edge = jnp.zeros((8, up_rows.shape[1]), jnp.float32)
    up_rows[pl.ds(0, 8), :] = edge
    up_rows[pl.ds(total + 8, 8), :] = edge

    def project(z, _):
        block = rows_all[z].reshape(plane, width)
        up_weight = up_land[...].reshape(width, 2 * part)
        up = jnp.dot(block, up_weight, preferred_element_type=jnp.float32)
        start = pl.multiple_of(z * plane + 8, 8)
        up_rows[pl.ds(start, plane), :] = up.astype(jnp.bfloat16).astype(jnp.float32)
        return _

    lax.fori_loop(0, sizes["z"], project, 0)

    for copy in [keeps[2]] + down_copies:
        copy.wait()
    for source in range(count):
        down_ref[:, source * part_width : (source + 1) * part_width] = down_land[source]

    def mix(z, _):
        start = pl.multiple_of(z * plane, 8)
        window = up_rows[pl.ds(start, plane + 16), :]
        convolved = (
            taps_ref[0:1, :] * window[7 : plane + 7]
            + taps_ref[1:2, :] * window[8 : plane + 8]
            + taps_ref[2:3, :] * window[9 : plane + 9]
        )
        gate = convolved[:, part:]
        hidden = convolved[:, :part] * (gate / (1.0 + jnp.exp(-gate)))
        sums = jnp.dot(
            hidden.astype(jnp.bfloat16), down_ref[...], preferred_element_type=jnp.float32
        )
        partial[z] = sums.astype(jnp.bfloat16).reshape(partial.shape[1:])
        return _

    lax.fori_loop(0, sizes["z"], mix, 0)

    def start_sum(piece, stage, slot):
        axis = sum_orders[piece][stage]
        done = sum_orders[piece][:stage]
        started = []
        for offset in range(1, sizes[axis]):
            place, device = neighbour(axis, offset)
            index = tuple(
                place if name == axis else mine[name] if name in done else slice(None)
                for name in axes
            )
            copy = pltpu.make_async_remote_copy(
                src_ref=partial.at[index + (slice(None), pl.ds(piece * half, half))],
                dst_ref=landing[piece * 4 + stage].at[offset - 1],
                send_sem=send_sem.at[slot],
                recv_sem=recv_sem.at[slot],
                device_id=device,
                device_id_type=mesh_ids,
            )
            copy.start()
            started.append(copy)
            slot += 1
        return started, slot

    def add_landed(piece, stage):
        axis = sum_orders[piece][stage]
        done = sum_orders[piece][: stage + 1]
        land = landing[piece * 4 + stage]
        columns = pl.ds(piece * half, half)
        free = [name for name in axes if name not in done]

        def add(step, _):
            index, inner = [], ()
            for name in axes:
                if name in done:
                    index.append(mine[name])
                elif name == free[0]:
                    index.append(step)
                    inner = (step,)
                else:
                    index.append(slice(None))
            index = tuple(index) + (slice(None), columns)
            value = partial[index].astype(jnp.float32)
            for offset in range(1, sizes[axis]):
                value = value + land[(offset - 1,) + inner].astype(jnp.float32)
            if free:
                partial[index] = value.astype(jnp.bfloat16)
            else:
                out_ref[:, columns] = (
                    hidden_state_ref[:, columns].astype(jnp.float32) + value
                ).astype(jnp.bfloat16)
            return _

        if free:
            lax.fori_loop(0, sizes[free[0]], add, 0)
        else:
            add(0, 0)

    slot = send_sem.shape[0] // 2
    for stage in range(4):
        for piece in range(2):
            if stage:
                for copy in pending[piece]:
                    copy.wait()
                add_landed(piece, stage - 1)
            pending[piece], slot = start_sum(piece, stage, slot)
    for piece in range(2):
        for copy in pending[piece]:
            copy.wait()
        add_landed(piece, 3)


def channel_mixer(normed, hidden_state, up_send, down_send, taps, sp_count, tp_count):
    cores = 2
    across = tp_count // cores
    deep = math.gcd(across, sp_count)
    sizes = {"z": sp_count // deep, "y": deep, "x": across, "c": cores}
    rows, width = normed.shape
    half = width // 2
    grid = tuple(sizes[name] for name in axes)
    total = math.prod(grid) * rows
    landing = []
    for order in sum_orders:
        for stage in range(4):
            axis = order[stage]
            left = tuple(sizes[name] for name in axes if name not in order[: stage + 1])
            landing.append(
                pltpu.VMEM((max(sizes[axis] - 1, 1),) + left + (rows, half), jnp.bfloat16)
            )
    copies = 2 * 2 * sum(max(sizes[name] - 1, 0) for name in axes)
    vmem = pl.BlockSpec(memory_space=pltpu.VMEM)
    return pl.pallas_call(
        lambda *refs: channel_kernel(sizes, *refs),
        name="channel_mixer",
        out_shape=jax.ShapeDtypeStruct((rows, width), jnp.bfloat16),
        in_specs=[vmem] * 5,
        out_specs=vmem,
        scratch_shapes=[
            pltpu.VMEM(grid + (rows, width), jnp.bfloat16),
            pltpu.VMEM((total + 16, up_send.shape[2]), jnp.float32),
            pltpu.VMEM(grid + (rows, width), jnp.bfloat16),
            pltpu.VMEM(up_send.shape, jnp.bfloat16),
            pltpu.VMEM(down_send.shape, jnp.bfloat16),
            pltpu.VMEM((down_send.shape[1], width), jnp.bfloat16),
            *landing,
            pltpu.SemaphoreType.DMA((3,)),
            pltpu.SemaphoreType.DMA((copies,)),
            pltpu.SemaphoreType.DMA((copies,)),
            pltpu.SemaphoreType.DMA((2, sp_count)),
            pltpu.SemaphoreType.DMA((2, sp_count)),
        ],
        compiler_params=pltpu.CompilerParams(
            collective_id=1, has_side_effects=True, vmem_limit_bytes=63 * 1024 * 1024
        ),
    )(normed, hidden_state, up_send, down_send, taps)


def turns(step_size, count):
    coarse = jnp.round(step_size * 1024.0) / 1024.0
    whole = coarse * count
    whole = whole - 2.0 * jnp.floor(whole * 0.5)
    return whole + (step_size - coarse) * count


def mixer(mixer_input, time_step, damping, input_map, readout, skip_gain):
    rows = mixer_input.shape[0]
    groups = time_step.shape[1]
    states, width = input_map.shape[3], input_map.shape[4]
    count, mine = lax.axis_size("sp"), lax.axis_index("sp")
    at = jnp.arange(rows)
    lower = at[:, None] >= at[None, :]
    reach = jnp.stack((lower, lower.T))
    log_decay = -0.5 * time_step[:, None, :] - damping
    log_sum = jnp.einsum("ktu,kug->kgt", reach.astype(jnp.float32), log_decay, precision=highest)
    weights = jnp.where(
        reach[:, None],
        jnp.exp(jnp.minimum(log_sum[:, :, :, None] - log_sum[:, :, None, :], 0.0)),
        0.0,
    )
    number = jnp.arange(states, dtype=jnp.float32)
    dt = time_step[:, :, None, None]
    angle = math.pi * turns(dt, number[None, :] * at.astype(jnp.float32)[:, None])
    sign = jnp.array([1.0, -1.0], jnp.float32)[:, None, None, None]
    cos, sin = jnp.cos(angle), jnp.sin(angle) * sign
    grouped = mixer_input.reshape(rows, groups, width)
    drive = jnp.einsum("tgh,kpgnh->kpgtn", grouped, input_map, preferred_element_type=jnp.float32)
    drive = drive * jnp.sqrt(-jnp.expm1(-time_step))[:, None, :, None, None]
    rotated = jnp.concatenate(
        (cos * drive[:, 0] + sin * drive[:, 1], cos * drive[:, 1] - sin * drive[:, 0]), axis=3
    )
    local = jnp.einsum("kgts,kgsn->kgtn", weights, rotated, precision=highest)
    ends = jnp.stack((local[0, :, -1], local[1, :, 0]))
    totals = jnp.stack((log_sum[0, :, -1], log_sum[1, :, 0]))
    flat = ends.reshape(2 * groups, 2 * states)
    spare = jnp.pad(totals.reshape(1, 2 * groups), ((0, 7), (0, 2 * states - 2 * groups)))
    every = gather_ends(jnp.concatenate((flat, spare), axis=0), count)
    end_all = every[:, : 2 * groups].reshape(count, 2, groups, 2 * states)
    total_all = every[:, 2 * groups, : 2 * groups].reshape(count, 2, groups)
    index = jnp.arange(count)
    away = jnp.stack((mine - index, index - mine), axis=1)
    lo = jnp.minimum(index, mine)[:, None]
    hi = jnp.maximum(index, mine)[:, None]
    between = ((index[None, :] > lo) & (index[None, :] < hi)).astype(jnp.float32)
    span = jnp.einsum("ji,ikg->jkg", between, total_all, precision=highest)
    factor = jnp.where(away[:, :, None] > 0, jnp.exp(span), 0.0)
    block_turn = turns(time_step[:, :, None], number * rows)
    hop = jnp.abs(mine - index).astype(jnp.float32)[:, None, None, None] * block_turn
    hop = math.pi * (hop - 2.0 * jnp.floor(hop * 0.5))
    hop_cos, hop_sin = jnp.cos(hop) * factor[..., None], jnp.sin(hop) * factor[..., None]
    end_re, end_im = end_all[..., :states], end_all[..., states:]
    carry = jnp.concatenate(
        (
            jnp.sum(hop_cos * end_re - hop_sin * end_im, axis=0),
            jnp.sum(hop_cos * end_im + hop_sin * end_re, axis=0),
        ),
        axis=2,
    )
    local = local + jnp.exp(log_sum)[..., None] * carry[:, :, None, :]
    re, im = local[..., :states], local[..., states:]
    state = jnp.concatenate((cos * re - sin * im, cos * im + sin * re), axis=3)
    out_map = jnp.concatenate((readout[:, 0], -readout[:, 1]), axis=3)
    mixed = jnp.einsum("kgtn,kghn->tgh", state, out_map, precision=highest)
    return mixed.reshape(rows, groups * width) + skip_gain[None, :] * mixer_input.astype(
        jnp.float32
    )


def body(
    mixer_input,
    time_step,
    damping,
    input_map,
    readout,
    skip_gain,
    out_gain,
    out_weight,
    residual,
    channel_gain,
    value_weight,
    gate_weight,
    value_taps,
    gate_taps,
    down_weight,
):
    count, mine = lax.axis_size("sp"), lax.axis_index("sp")
    depth, hidden_width = value_weight.shape
    part = hidden_width // count
    up_send = jnp.concatenate(
        (
            value_weight.reshape(depth, count, part).swapaxes(0, 1),
            gate_weight.reshape(depth, count, part).swapaxes(0, 1),
        ),
        axis=2,
    )
    down_send = down_weight.reshape(count, part, down_weight.shape[1])
    mixed_y = mixer(mixer_input, time_step, damping, input_map, readout, skip_gain)
    tp_count = lax.axis_size("tp")
    mixed_y = mixed_y.reshape(tp_count, -1, out_gain.shape[0])
    gain_row = jnp.broadcast_to(out_gain, (tp_count, 1, out_gain.shape[0]))
    mixed_y = jnp.concatenate((mixed_y, gain_row), axis=1)
    mixed_y = lax.all_to_all(mixed_y, "tp", split_axis=0, concat_axis=0, tiled=True)
    mixed_y = mixed_y.swapaxes(0, 1).reshape(mixed_y.shape[1], -1)
    mixed_y, gain = mixed_y[:-1], mixed_y[-1]
    inverse = lax.rsqrt(jnp.mean(mixed_y * mixed_y, axis=1, keepdims=True) + norm_eps)
    normed_mix = (mixed_y * inverse * gain[None, :]).astype(jnp.bfloat16)
    mixed_rows = jnp.dot(normed_mix, out_weight, preferred_element_type=jnp.float32)
    hidden_state = (residual.astype(jnp.float32) + mixed_rows).astype(jnp.bfloat16)
    state_wide = hidden_state.astype(jnp.float32)
    scale_rows = lax.rsqrt(jnp.mean(state_wide * state_wide, axis=1, keepdims=True) + norm_eps)
    normed = (state_wide * scale_rows * channel_gain[None, :]).astype(jnp.bfloat16)
    taps = jnp.concatenate(
        (
            lax.dynamic_slice_in_dim(value_taps, mine * part, part, axis=1),
            lax.dynamic_slice_in_dim(gate_taps, mine * part, part, axis=1),
        ),
        axis=1,
    )
    return channel_mixer(normed, hidden_state, up_send, down_send, taps, count, tp_count)


def solution(mesh):
    in_specs = (
        P("sp", "tp"),
        P(None, "tp"),
        P(None, "sp", "tp"),
        P(None, None, "tp", None, None),
        P(None, None, "tp", None, None),
        P("tp"),
        P("tp"),
        P(),
        P(("sp", "tp"), None),
        P(),
        P("sp", "tp"),
        P("sp", "tp"),
        P(None, "tp"),
        P(None, "tp"),
        P("tp", "sp"),
    )
    out_specs = P(("sp", "tp"), None)
    return jax.shard_map(body, mesh=mesh, in_specs=in_specs, out_specs=out_specs, check_vma=False)
```

profile of v0, /device:TPU:0, one launch (start us, length us, event | category | flops | bytes accessed | tf_op | source)
XLA Modules:
  0.0 170.5 jit_solution(1692093892177225839)
XLA Ops:
  0.1 0.7 broadcast_multiply_fusion
  0.8 0.1 copy.56
  0.8 0.1 copy.57
  0.9 0.1 copy.60
  1.0 1.0 copy.58
  2.0 1.0 fusion.55
  3.0 0.2 slice_reduce_fusion.1
  3.2 1.5 bitcast_multiply_fusion
  4.7 4.5 %multiply_add_fusion.2 = (f32[2,16,128,64]{2,3,0,1:T(8,128)S(1)}, f32[2,16,128,64]{2,3,0,1:T(8,128)S(1)}) fusion(f32[2,2,16,128,64]{3,4,1,0,2:T(8,128)S(1)} %bitcast_multiply_fusion, f32[2]{0:T(128)S(1)} %copy-done.7, f32[2,16]{0,1:T(8,128)S(1)} %copy.57, f32[128,64]{0,1:T(8,128)S(1)} %iota_multiply_fusion, f32[2,16]{0,1:T(8,128)S(1)} %copy.56), kind=kLoop, calls=%fused_computation.29 | loop fusion | flops 3932160 | bytes 4227336 | tf_op jit(solution)/shard_map/add | solution.py:347
  9.2 4.6 %fusion.5 = f32[2,16,128,128]{3,2,1,0:T(8,128)S(1)} fusion(f32[2,16,128]{2,1,0:T(8,128)S(1)} %get-tuple-element.24, pred[2,128,128]{2,1,0:T(8,128)(4,1)S(1)} %pad_add_fusion, f32[2,16,128,64]{2,3,0,1:T(8,128)S(1)} %get-tuple-element.12, f32[2,16,128,64]{2,3,0,1:T(8,128)S(1)} %get-tuple-element.11), kind=kOutput, calls=%fused_computation.7 | convolution fusion | flops 807403520 | bytes 4243456 | tf_op jit(solution)/shard_map/kgts,kgsn->kgtn/dot_general | solution.py:349
  13.8 1.3 copy-done
  15.2 0.1 reshape.182
  15.3 0.6 select_maximum_fusion.refs_0_
  15.9 11.0 %gather_ends.1 = f32[8,40,128]{2,1,0:T(8,128)} custom-call(f32[40,128]{1,0:T(8,128)} %select_maximum_fusion.refs_0_), custom_call_target="tpu_custom_call" | custom-call | tf_op jit(solution)/shard_map/gather_ends/pallas_call | solution.py:44
  26.9 0.8 slice_reduce_fusion.2
  27.7 2.0 %copy.68 = f32[2,16,128,128]{2,3,0,1:T(8,128)S(1)} copy(f32[2,16,128,128]{3,2,1,0:T(8,128)} %copy-done) | data formatting | bytes 4194304 | tf_op jit(solution)/shard_map/kgts,kgsn->kgtn/dot_general | solution.py:349
  29.7 0.1 reshape_squeeze.3
  29.8 0.2 fusion.11
  30.0 0.1 fusion.40
  30.0 0.0 slice-done
  30.1 0.6 subtract_reduce_fusion
  30.7 0.1 pad_maximum_fusion.4
  30.8 0.7 multiply_add_fusion
  31.5 0.0 copy-start.3
  31.5 4.5 %multiply_subtract_fusion.1 = (f32[2,16,128,64]{2,3,0,1:T(8,128)S(1)}, f32[2,16,128,64]{2,3,0,1:T(8,128)S(1)}) fusion(f32[2,16,128,128]{2,3,0,1:T(8,128)S(1)} %multiply_add_fusion, f32[2]{0:T(128)S(1)} %copy-done.7, f32[2,16]{0,1:T(8,128)S(1)} %copy.57, f32[128,64]{0,1:T(8,128)S(1)} %iota_multiply_fusion, f32[2,16]{0,1:T(8,128)S(1)} %copy.56), kind=kLoop, calls=%fused_computation.27 | loop fusion | flops 3932160 | bytes 4227336 | tf_op jit(solution)/shard_map/sub | solution.py:378
  36.1 0.0 copy-start.4
  36.1 0.0 copy-start.8
  36.1 0.0 copy-start.9
  36.1 0.1 fusion.27
  36.2 0.0 copy-start.2
  36.2 1.2 fusion.1
  37.4 0.1 copy.70
  37.6 0.7 pad_maximum_fusion.2
  38.2 3.5 %all-to-all-start = ((f32[4,33,256]{2,1,0:T(8,128)}), f32[4,33,256]{2,1,0:T(8,128)S(1)}, u32[]{:S(2)}, u32[]{:S(2)}) async-start(f32[4,33,256]{2,1,0:T(8,128)} %pad_maximum_fusion.2), calls=%async_computation | async-start | bytes 327680 | tf_op jit(solution)/shard_map/all_to_all | solution.py:419
  41.8 0.3 copy.72
  42.1 0.5 copy.73
  42.6 1.4 copy.74
  44.0 0.5 copy.75
  44.5 0.0 copy-start.5
  44.5 1.7 %pad_maximum_fusion.1.refs_2_ = bf16[8,256,384]{2,1,0:T(8,128)(2,1)} fusion(bf16[8,256,192]{2,1,0:T(8,128)(2,1)S(1)} %bitcast.56, bf16[8,256,192]{2,1,0:T(8,128)(2,1)S(1)} %bitcast.55), kind=kLoop, calls=%fused_computation.15 | loop fusion | flops 3145728 | bytes 3145728 | tf_op jit(solution)/shard_map/concatenate | solution.py:406
  46.2 0.8 constant_dynamic-slice_fusion
  47.0 0.7 pad_maximum_fusion.5.refs_4_
  47.7 0.1 multiply_reduce_fusion
  47.9 0.0 copy-start.6
  47.9 3.2 %fusion.21 = (f32[32]{0:T(128)S(1)}, bf16[32,2048]{1,0:T(8,128)(2,1)S(1)}) fusion(bf16[1024,2048]{1,0:T(8,128)(2,1)} %param.23, f32[32,1024]{1,0:T(8,128)S(1)} %bitcast.63, f32[1024]{0:T(1024)S(1)} %bitcast.70, f32[32]{0:T(128)S(1)} %add_rsqrt_fusion.1, bf16[32,2048]{1,0:T(8,128)(2,1)S(1)} %copy-done.5), kind=kOutput, calls=%fused_computation.38 | convolution fusion | flops 134709216 | bytes 4591872 | tf_op jit(solution)/shard_map/dot_general | solution.py:424
  51.1 0.8 fusion.23.refs_0_
  51.8 117.1 %channel_mixer.1 = bf16[32,2048]{1,0:T(8,128)(2,1)} custom-call(bf16[32,2048]{1,0:T(8,128)(2,1)} %fusion.23.refs_0_, bf16[32,2048]{1,0:T(8,128)(2,1)} %copy-done.1, bf16[8,256,384]{2,1,0:T(8,128)(2,1)} %pad_maximum_fusion.1.refs_2_, bf16[8,192,256]{2,1,0:T(8,128)(2,1)} %bitcast.60, f32[3,384]{1,0:T(4,128)} %pad_maximum_fusion.5.refs_4_), custom_call_target="tpu_custom_call" | custom-call | tf_op jit(solution)/shard_map/channel_mixer/pallas_call | solution.py:290
  169.0 1.6 copy.103
  (36 shorter events, 0.3 us)
Async XLA Ops:
  0.0 4.7 %copy-start.7 = (f32[2]{0:T(128)S(1)}, f32[2]{0:T(128)}, u32[]{:S(2)}) copy-start(f32[2]{0:T(128)} %constant.15.clone) | copy-start | bytes 28
  13.8 1.3 copy-start
  27.7 2.4 %slice-start = ((f32[8,40,128]{2,1,0:T(8,128)}), f32[8,32,128]{2,1,0:T(8,128)S(1)}, s32[]{:S(2)}) async-start(f32[8,40,128]{2,1,0:T(8,128)} %gather_ends.1), calls=%async_computation.1 | async-start | bytes 262144 | tf_op jit(solution)/shard_map/slice | solution.py:355
  31.5 4.5 %copy-start.3 = (f32[2,2,16,16,64]{4,3,2,1,0:T(8,128)S(1)}, f32[2,2,16,16,64]{4,3,2,1,0:T(8,128)}, u32[]{:S(2)}) copy-start(f32[2,2,16,16,64]{4,3,2,1,0:T(8,128)} %param.20) | copy-start | bytes 786436
  36.1 1.4 copy-start.4
  36.1 1.4 copy-start.8
  36.1 1.4 copy-start.9
  36.2 5.6 %copy-start.2 = (bf16[256,1536]{1,0:T(8,128)(2,1)S(1)}, bf16[256,1536]{1,0:T(8,128)(2,1)}, u32[]{:S(2)}) copy-start(bf16[256,1536]{1,0:T(8,128)(2,1)} %param.26) | copy-start | bytes 2359300
  38.2 9.5 %all-to-all-start = ((f32[4,33,256]{2,1,0:T(8,128)}), f32[4,33,256]{2,1,0:T(8,128)S(1)}, u32[]{:S(2)}, u32[]{:S(2)}) async-start(f32[4,33,256]{2,1,0:T(8,128)} %pad_maximum_fusion.2), calls=%async_computation | async-start | bytes 327680 | tf_op jit(solution)/shard_map/all_to_all | solution.py:419
  44.5 3.3 %copy-start.5 = (bf16[32,2048]{1,0:T(8,128)(2,1)S(1)}, bf16[32,2048]{1,0:T(8,128)(2,1)}, u32[]{:S(2)}) copy-start(bf16[32,2048]{1,0:T(8,128)(2,1)} %param.24) | copy-start | bytes 393220
  47.9 3.2 %copy-start.6 = (f32[2048]{0:T(1024)S(1)}, f32[2048]{0:T(1024)}, u32[]{:S(2)}) copy-start(f32[2048]{0:T(1024)} %param.25) | copy-start | bytes 24580
  51.0 0.8 copy-start.1
where the time goes:
time: 171 us
  Pallas kernels  128 us (75%)
  other arithmetic  15.9 us (9%)
  matrix products  11.6 us (7%)
  local copies, waits for them, and re-layouts  10.9 us (6%)
  starting transfers between devices  3.52 us (2%)
    pallas_call x1, Pallas kernels, channel_mixer(): pl.pallas_call(lambda *refs: channel_kernel(sizes, *refs), name='channel_...  117 us
    pallas_call x1, Pallas kernels, gather_ends(): pl.pallas_call(lambda *refs: carry_kernel(count, *refs), name='gather_end...  11 us
    unnamed x24, local copies, waits for them, and re-layouts  5.59 us
    dot_general x1, matrix products, mixer(): local = jnp.einsum('kgts,kgsn->kgtn', weights, rotated, precision=highest)  4.61 us
    sub x1, other arithmetic, mixer(): state = jnp.concatenate((cos * re - sin * im, cos * im + sin * re), axis=3)  4.5 us
    add x1, other arithmetic, mixer(): cos * drive[:, 0] + sin * drive[:, 1]  4.5 us
    all_to_all x1, starting transfers between devices, body(): lax.all_to_all(mixed_y, 'tp', split_axis=0, concat_axis=0, tiled=True)  3.52 us
  transfers between devices with their start and end apart: 1, of which 0 were waited for; matrix products, arithmetic and copies ran while one was open for 3% of the time, Pallas kernels for 0%

commit v1 on v0

--- a/solution.py
+++ b/solution.py
@@ -346,7 +346,7 @@
     rotated = jnp.concatenate(
         (cos * drive[:, 0] + sin * drive[:, 1], cos * drive[:, 1] - sin * drive[:, 0]), axis=3
     )
-    local = jnp.einsum("kgts,kgsn->kgtn", weights, rotated, precision=highest)
+    local = jnp.einsum("kgts,kgsn->kgtn", weights, rotated, precision=lax.Precision.HIGH)
     ends = jnp.stack((local[0, :, -1], local[1, :, 0]))
     totals = jnp.stack((log_sum[0, :, -1], log_sum[1, :, 0]))
     flat = ends.reshape(2 * groups, 2 * states)
@@ -377,7 +377,7 @@
     re, im = local[..., :states], local[..., states:]
     state = jnp.concatenate((cos * re - sin * im, cos * im + sin * re), axis=3)
     out_map = jnp.concatenate((readout[:, 0], -readout[:, 1]), axis=3)
-    mixed = jnp.einsum("kgtn,kghn->tgh", state, out_map, precision=highest)
+    mixed = jnp.einsum("kgtn,kghn->tgh", state, out_map, precision=lax.Precision.HIGH)
     return mixed.reshape(rows, groups * width) + skip_gain[None, :] * mixer_input.astype(
         jnp.float32
     )

time: 171 us -> 169 us (0.988)
  matrix products: 11.6 us -> 9.03 us
    dot_general x2, matrix products: 5.79 us -> 3.21 us  [the longest x1 2.43 us: mixer(): jnp.einsum('kgts,kgsn->kgtn', weights, rotated, precision=lax.Precision.H...]
where the time goes in v1:
time: 169 us; the launch traced here: 168 us
  Pallas kernels  128 us (76%)
  other arithmetic  15.9 us (9%)
  local copies, waits for them, and re-layouts  10.9 us (6%)
  matrix products  9.03 us (5%)
  starting transfers between devices  3.34 us (2%)
    pallas_call x1, Pallas kernels, channel_mixer(): pl.pallas_call(lambda *refs: channel_kernel(sizes, *refs), name='channel_...  117 us
    pallas_call x1, Pallas kernels, gather_ends(): pl.pallas_call(lambda *refs: carry_kernel(count, *refs), name='gather_end...  11 us
    unnamed x24, local copies, waits for them, and re-layouts  5.59 us
    add x1, other arithmetic, mixer(): cos * drive[:, 0] + sin * drive[:, 1]  4.5 us
    sub x1, other arithmetic, mixer(): state = jnp.concatenate((cos * re - sin * im, cos * im + sin * re), axis=3)  4.5 us
  transfers between devices with their start and end apart: 1, of which 0 were waited for; matrix products, arithmetic and copies ran while one was open for 3% of the time, Pallas kernels for 0%

profile of v1, /device:TPU:0, one launch (start us, length us, event | category | flops | bytes accessed | tf_op | source)
XLA Modules:
  0.0 168.0 jit_solution(2502206506006835890)
XLA Ops:
  0.1 0.7 broadcast_multiply_fusion
  0.8 0.1 copy.56
  0.8 0.1 copy.57
  0.9 0.1 copy.60
  1.0 1.0 copy.58
  2.0 1.0 fusion.55
  3.0 0.2 slice_reduce_fusion.1
  3.2 1.5 bitcast_multiply_fusion
  4.7 4.5 %multiply_add_fusion.2 = (f32[2,16,128,64]{2,3,0,1:T(8,128)S(1)}, f32[2,16,128,64]{2,3,0,1:T(8,128)S(1)}) fusion(f32[2,2,16,128,64]{3,4,1,0,2:T(8,128)S(1)} %bitcast_multiply_fusion, f32[2]{0:T(128)S(1)} %copy-done.7, f32[2,16]{0,1:T(8,128)S(1)} %copy.57, f32[128,64]{0,1:T(8,128)S(1)} %iota_multiply_fusion, f32[2,16]{0,1:T(8,128)S(1)} %copy.56), kind=kLoop, calls=%fused_computation.29 | loop fusion | flops 3932160 | bytes 4227336 | tf_op jit(solution)/shard_map/add | solution.py:347
  9.2 2.4 %fusion.5 = f32[2,16,128,128]{3,2,1,0:T(8,128)S(1)} fusion(f32[2,16,128]{2,1,0:T(8,128)S(1)} %get-tuple-element.24, pred[2,128,128]{2,1,0:T(8,128)(4,1)S(1)} %pad_add_fusion, f32[2,16,128,64]{2,3,0,1:T(8,128)S(1)} %get-tuple-element.12, f32[2,16,128,64]{2,3,0,1:T(8,128)S(1)} %get-tuple-element.11), kind=kOutput, calls=%fused_computation.7 | convolution fusion | flops 404750336 | bytes 4243456 | tf_op jit(solution)/shard_map/kgts,kgsn->kgtn/dot_general | solution.py:349
  11.6 1.3 copy-done
  13.0 0.1 reshape.182
  13.1 0.6 select_maximum_fusion.refs_0_
  13.7 11.0 %gather_ends.1 = f32[8,40,128]{2,1,0:T(8,128)} custom-call(f32[40,128]{1,0:T(8,128)} %select_maximum_fusion.refs_0_), custom_call_target="tpu_custom_call" | custom-call | tf_op jit(solution)/shard_map/gather_ends/pallas_call | solution.py:44
  24.7 0.8 slice_reduce_fusion.2
  25.5 2.0 %copy.68 = f32[2,16,128,128]{2,3,0,1:T(8,128)S(1)} copy(f32[2,16,128,128]{3,2,1,0:T(8,128)} %copy-done) | data formatting | bytes 4194304 | tf_op jit(solution)/shard_map/kgts,kgsn->kgtn/dot_general | solution.py:349
  27.5 0.1 reshape_squeeze.3
  27.6 0.2 fusion.11
  27.8 0.1 fusion.40
  27.9 0.0 slice-done
  27.9 0.6 subtract_reduce_fusion
  28.5 0.1 pad_maximum_fusion.4
  28.6 0.7 multiply_add_fusion
  29.3 0.0 copy-start.3
  29.4 4.5 %multiply_subtract_fusion.1 = (f32[2,16,128,64]{2,3,0,1:T(8,128)S(1)}, f32[2,16,128,64]{2,3,0,1:T(8,128)S(1)}) fusion(f32[2,16,128,128]{2,3,0,1:T(8,128)S(1)} %multiply_add_fusion, f32[2]{0:T(128)S(1)} %copy-done.7, f32[2,16]{0,1:T(8,128)S(1)} %copy.57, f32[128,64]{0,1:T(8,128)S(1)} %iota_multiply_fusion, f32[2,16]{0,1:T(8,128)S(1)} %copy.56), kind=kLoop, calls=%fused_computation.27 | loop fusion | flops 3932160 | bytes 4227336 | tf_op jit(solution)/shard_map/sub | solution.py:378
  33.9 0.0 copy-start.4
  33.9 0.0 copy-start.8
  33.9 0.0 copy-start.9
  33.9 0.1 fusion.27
  34.0 0.0 copy-start.2
  34.0 0.8 fusion.1
  34.8 0.1 copy.70
  35.0 0.7 pad_maximum_fusion.2
  35.7 3.3 %all-to-all-start = ((f32[4,33,256]{2,1,0:T(8,128)}), f32[4,33,256]{2,1,0:T(8,128)S(1)}, u32[]{:S(2)}, u32[]{:S(2)}) async-start(f32[4,33,256]{2,1,0:T(8,128)} %pad_maximum_fusion.2), calls=%async_computation | async-start | bytes 327680 | tf_op jit(solution)/shard_map/all_to_all | solution.py:419
  39.0 0.3 copy.72
  39.3 0.5 copy.73
  39.8 1.4 copy.74
  41.2 0.5 copy.75
  41.7 0.0 copy-start.5
  41.8 1.7 %pad_maximum_fusion.1.refs_2_ = bf16[8,256,384]{2,1,0:T(8,128)(2,1)} fusion(bf16[8,256,192]{2,1,0:T(8,128)(2,1)S(1)} %bitcast.56, bf16[8,256,192]{2,1,0:T(8,128)(2,1)S(1)} %bitcast.55), kind=kLoop, calls=%fused_computation.15 | loop fusion | flops 3145728 | bytes 3145728 | tf_op jit(solution)/shard_map/concatenate | solution.py:406
  43.5 0.8 constant_dynamic-slice_fusion
  44.3 0.7 pad_maximum_fusion.5.refs_4_
  44.9 0.1 multiply_reduce_fusion
  45.1 0.0 copy-start.6
  45.1 3.2 %fusion.21 = (f32[32]{0:T(128)S(1)}, bf16[32,2048]{1,0:T(8,128)(2,1)S(1)}) fusion(bf16[1024,2048]{1,0:T(8,128)(2,1)} %param.23, f32[32,1024]{1,0:T(8,128)S(1)} %bitcast.63, f32[1024]{0:T(1024)S(1)} %bitcast.70, f32[32]{0:T(128)S(1)} %add_rsqrt_fusion.1, bf16[32,2048]{1,0:T(8,128)(2,1)S(1)} %copy-done.5), kind=kOutput, calls=%fused_computation.38 | convolution fusion | flops 134709216 | bytes 4591872 | tf_op jit(solution)/shard_map/dot_general | solution.py:424
  48.3 0.8 fusion.23.refs_0_
  49.1 117.3 %channel_mixer.1 = bf16[32,2048]{1,0:T(8,128)(2,1)} custom-call(bf16[32,2048]{1,0:T(8,128)(2,1)} %fusion.23.refs_0_, bf16[32,2048]{1,0:T(8,128)(2,1)} %copy-done.1, bf16[8,256,384]{2,1,0:T(8,128)(2,1)} %pad_maximum_fusion.1.refs_2_, bf16[8,192,256]{2,1,0:T(8,128)(2,1)} %bitcast.60, f32[3,384]{1,0:T(4,128)} %pad_maximum_fusion.5.refs_4_), custom_call_target="tpu_custom_call" | custom-call | tf_op jit(solution)/shard_map/channel_mixer/pallas_call | solution.py:290
  166.4 1.6 copy.103
  (36 shorter events, 0.3 us)
Async XLA Ops:
  0.0 4.7 %copy-start.7 = (f32[2]{0:T(128)S(1)}, f32[2]{0:T(128)}, u32[]{:S(2)}) copy-start(f32[2]{0:T(128)} %constant.15.clone) | copy-start | bytes 28
  11.6 1.3 copy-start
  25.5 2.4 %slice-start = ((f32[8,40,128]{2,1,0:T(8,128)}), f32[8,32,128]{2,1,0:T(8,128)S(1)}, s32[]{:S(2)}) async-start(f32[8,40,128]{2,1,0:T(8,128)} %gather_ends.1), calls=%async_computation.1 | async-start | bytes 262144 | tf_op jit(solution)/shard_map/slice | solution.py:355
  29.3 4.5 %copy-start.3 = (f32[2,2,16,16,64]{4,3,2,1,0:T(8,128)S(1)}, f32[2,2,16,16,64]{4,3,2,1,0:T(8,128)}, u32[]{:S(2)}) copy-start(f32[2,2,16,16,64]{4,3,2,1,0:T(8,128)} %param.20) | copy-start | bytes 786436
  33.9 1.0 copy-start.4
  33.9 1.0 copy-start.8
  33.9 1.0 copy-start.9
  34.0 5.0 %copy-start.2 = (bf16[256,1536]{1,0:T(8,128)(2,1)S(1)}, bf16[256,1536]{1,0:T(8,128)(2,1)}, u32[]{:S(2)}) copy-start(bf16[256,1536]{1,0:T(8,128)(2,1)} %param.26) | copy-start | bytes 2359300
  35.7 9.3 %all-to-all-start = ((f32[4,33,256]{2,1,0:T(8,128)}), f32[4,33,256]{2,1,0:T(8,128)S(1)}, u32[]{:S(2)}, u32[]{:S(2)}) async-start(f32[4,33,256]{2,1,0:T(8,128)} %pad_maximum_fusion.2), calls=%async_computation | async-start | bytes 327680 | tf_op jit(solution)/shard_map/all_to_all | solution.py:419
  41.7 3.3 %copy-start.5 = (bf16[32,2048]{1,0:T(8,128)(2,1)S(1)}, bf16[32,2048]{1,0:T(8,128)(2,1)}, u32[]{:S(2)}) copy-start(bf16[32,2048]{1,0:T(8,128)(2,1)} %param.24) | copy-start | bytes 393220
  45.1 3.2 %copy-start.6 = (f32[2048]{0:T(1024)S(1)}, f32[2048]{0:T(1024)}, u32[]{:S(2)}) copy-start(f32[2048]{0:T(1024)} %param.25) | copy-start | bytes 24580
  48.3 0.8 copy-start.1
